TPU v7x, 128 devices: a whole 4x4x4 slice. The times are simulated.
128 devices in a mesh: ep: 128 (over z, y, x, core).
Axes of the slice: x: 4, y: 4, z: 4, core: 2. Of those that a mesh axis runs over, the one named last changes fastest.
Arguments:
- tokens: bfloat16 [2048, 1024], P('ep'), may hold values from -6 to 6
- lengths: int32 [2048], P('ep'), may hold values from 1 to 8191
- cache_keys: bfloat16 [2048, 128, 512], P('ep'), may hold values from -6 to 6
- cache_values: bfloat16 [2048, 128, 1024], P('ep'), may hold values from -6 to 6
- retention_state: float32 [2048, 4, 128, 256], P('ep'), may hold values from -24 to 24
- mix_gain: float32 [1024], replicated, may hold values from 0.1 to 1.9
- query_weight: bfloat16 [1024, 512], replicated, may hold values from -0.1875 to 0.1875
- key_weight: bfloat16 [1024, 512], replicated, may hold values from -0.1875 to 0.1875
- value_weight: bfloat16 [1024, 1024], replicated, may hold values from -0.1875 to 0.1875
- out_weight: bfloat16 [1024, 1024], replicated, may hold values from -0.1875 to 0.1875
- ffn_gain: float32 [1024], replicated, may hold values from 0.1 to 1.9
- routes: int32 [2048, 6], P('ep'), may hold values from 0 to 127, all different within a row; in each aligned block of 16 rows (0 to 15, 16 to 31, ...) at most 2 rows name the same one
- route_scores: float32 [2048, 6], P('ep'), may hold values from 0.05 to 1
- expert_gate: bfloat16 [128, 1024, 256], P('ep'), may hold values from -0.1875 to 0.1875
- expert_up: bfloat16 [128, 1024, 256], P('ep'), may hold values from -0.1875 to 0.1875
- expert_down: bfloat16 [128, 256, 1024], P('ep'), may hold values from -0.375 to 0.375
- shared_gate: bfloat16 [1024, 256], replicated, may hold values from -0.1875 to 0.1875
- shared_up: bfloat16 [1024, 256], replicated, may hold values from -0.1875 to 0.1875
- shared_down: bfloat16 [256, 1024], replicated, may hold values from -0.375 to 0.375
- dense_gate: bfloat16 [4096, 1024], P('ep'), may hold values from -0.1875 to 0.1875
- dense_up: bfloat16 [4096, 1024], P('ep'), may hold values from -0.1875 to 0.1875
- dense_down: bfloat16 [4096, 1024], P('ep'), may hold values from -0.09375 to 0.09375
- dense_mix: float32 [1024], replicated, may hold values from -3 to 3
Outputs:
- layer_out: bfloat16 [2048, 1024], P('ep')
- new_keys: bfloat16 [2048, 512], P('ep')
- new_values: bfloat16 [2048, 1024], P('ep')
Inputs may be any that keep to these rules, and one draw needn't show every extreme that they name: `routes`: each row names 6 different experts; among the rows of one device no expert is named more than 2 times.
All inputs are finite; a program needn't handle non-finite values.
Results may differ from a plain program's by a relative error of at most 0.012.
Values may be sent and summed in bfloat16 or wider, within the bound.
A program may use at most 128 MiB of HBM per device.

v0:
```python
import functools

import jax
import jax.numpy as jnp
from jax import lax
from jax.experimental import pallas as pl
from jax.experimental.pallas import tpu as pltpu
from jax.sharding import PartitionSpec as P

eps = 1e-06
route_scale = 2.5
rope_base = 10000.0


def normed(values):
    return values * lax.rsqrt(jnp.mean(values * values, axis=-1, keepdims=True) + eps)


def log_decay(head_count):
    return jnp.log1p(-jnp.exp2(-5.0 - jnp.arange(head_count, dtype=jnp.float32)))


def rotate(values, positions):
    half_size = values.shape[-1] // 2
    inverse = rope_base ** (-jnp.arange(half_size, dtype=jnp.float32) / half_size)
    angles = positions.astype(jnp.float32)[:, None, None] * inverse[None, None, :]
    cosine = jnp.cos(angles)
    sine_part = jnp.sin(angles)
    first_half = values[..., :half_size]
    second = values[..., half_size:]
    return jnp.concatenate(
        [first_half * cosine - second * sine_part, first_half * sine_part + second * cosine],
        axis=-1,
    )


def retain(
    tokens, lengths, mix_gain, w_query, w_key, w_value, w_out, cache_keys, cache_values, carry_state
):
    seq_count, head_count, key_size, value_size = carry_state.shape
    block_size = cache_keys.shape[1]
    widened = tokens.astype(jnp.float32)
    normal_in = (normed(widened) * mix_gain).astype(jnp.bfloat16)
    raw_query = jnp.dot(normal_in, w_query, preferred_element_type=jnp.float32).reshape(
        seq_count, head_count, key_size
    )
    raw_key = jnp.dot(normal_in, w_key, preferred_element_type=jnp.float32).reshape(
        seq_count, head_count, key_size
    )
    raw_value = jnp.dot(normal_in, w_value, preferred_element_type=jnp.float32).reshape(
        seq_count, head_count, value_size
    )
    queries = (rotate(raw_query, lengths) * key_size ** (-0.5)).astype(jnp.bfloat16)
    new_keys = rotate(raw_key, lengths).astype(jnp.bfloat16)
    new_values = raw_value.astype(jnp.bfloat16)
    filled = lengths % block_size
    decay_rate = log_decay(head_count)
    places = jnp.arange(block_size, dtype=jnp.int32)
    stored_keys = cache_keys.reshape(seq_count, block_size, head_count, key_size)
    stored_values = cache_values.reshape(seq_count, block_size, head_count, value_size)
    scores = jnp.einsum("shd,sjhd->shj", queries, stored_keys, preferred_element_type=jnp.float32)
    distance = jnp.maximum(filled[:, None] - places[None, :], 0).astype(jnp.float32)
    live_mask = places[None, :] < filled[:, None]
    weighted = jnp.where(
        live_mask[:, None, :],
        scores * jnp.exp(distance[:, None, :] * decay_rate[None, :, None]),
        0.0,
    ).astype(jnp.bfloat16)
    own_weight = jnp.sum(
        queries.astype(jnp.float32) * new_keys.astype(jnp.float32), axis=-1
    ).astype(jnp.bfloat16)
    inside = jnp.einsum(
        "shj,sjhe->she", weighted, stored_values, preferred_element_type=jnp.float32
    )
    inside = inside + own_weight.astype(jnp.float32)[:, :, None] * new_values.astype(jnp.float32)
    carried = jnp.einsum(
        "shd,shde->she", queries.astype(jnp.float32), carry_state, precision=lax.Precision.HIGHEST
    )
    carried = (
        carried
        * jnp.exp((filled.astype(jnp.float32)[:, None] + 1.0) * decay_rate[None, :])[:, :, None]
    )
    headed = (
        normed(inside + carried).astype(jnp.bfloat16).reshape(seq_count, head_count * value_size)
    )
    mixer_out = jnp.dot(headed, w_out, preferred_element_type=jnp.float32)
    residual = widened + normed(mixer_out)
    return (
        residual,
        new_keys.reshape(seq_count, head_count * key_size),
        new_values.reshape(seq_count, head_count * value_size),
    )


MESH = pl.DeviceIdType.MESH


def grid_of(count):
    cores = 2 if count % 2 == 0 else 1
    chips = count // cores
    x_size = max(d for d in range(1, chips + 1) if chips % d == 0 and d**3 <= chips)
    plane = chips // x_size
    y_size = max(d for d in range(1, plane + 1) if plane % d == 0 and d**2 <= plane)
    return plane // y_size, y_size, x_size, cores


def silu(values):
    return values * (1.0 / (1.0 + jnp.exp(-values)))


def dot(left, right):
    return jnp.dot(left, right, preferred_element_type=jnp.float32)


def dot_rows(left, right):
    return lax.dot_general(
        left, right, (((1,), (1,)), ((), ())), preferred_element_type=jnp.float32
    )


def ffn_kernel(
    dims,
    experts,
    features_ref,
    residual_ref,
    mix_ref,
    *refs,
):
    nz, ny, nx, nc = dims
    weight_refs = refs[:9]
    out_ref = refs[9]
    held = refs[10:19]
    (
        block,
        gathered,
        own_part,
        other_part,
        core_in,
        sum0,
        in1a,
        in1b,
        sum1a,
        sum1b,
        in2a,
        in2b,
        sum2,
        in3,
        local_sem,
        send_sem,
        recv_sem,
    ) = refs[19:]
    seq_count, width = features_ref.shape
    model = residual_ref.shape[1]
    half = nz // 2
    me = lax.axis_index("ep")
    c = lax.rem(me, nc)
    x = lax.rem(me // nc, nx)
    y = lax.rem(me // (nc * nx), ny)
    z = me // (nc * nx * ny)

    def at(z_at, y_at, x_at, c_at):
        return ((z_at * ny + y_at) * nx + x_at) * nc + c_at

    loads = [
        pltpu.make_async_copy(weight_refs[i], held[i], local_sem.at[i]) for i in range(9)
    ]
    for i in (6, 7, 8, 0, 1, 2, 3, 4, 5):
        loads[i].start()
    keep = pltpu.make_async_copy(features_ref, gathered.at[z, y, x, c], local_sem.at[9])
    keep.start()

    z_peers = [lax.rem(z + d, nz) for d in range(1, nz)]
    y_peers = [lax.rem(y + d, ny) for d in range(1, ny)]
    x_peers = [lax.rem(x + d, nx) for d in range(1, nx)]
    other = nc - 1 - c
    z_ids = [at(p, y, x, c) for p in z_peers]
    y_ids = [at(z, p, x, c) for p in y_peers]
    x_ids = [at(z, y, p, c) for p in x_peers]
    core_id = at(z, y, x, other)
    barrier = pltpu.get_barrier_semaphore()
    peers = z_ids + y_ids + x_ids + [core_id]
    for peer in peers:
        pl.semaphore_signal(barrier, inc=1, device_id=(peer,), device_id_type=MESH)
    pl.semaphore_wait(barrier, len(peers))

    sems = iter(range(1000))

    def copy(src, dst, peer):
        slot = next(sems)
        made = pltpu.make_async_remote_copy(
            src_ref=src,
            dst_ref=dst,
            send_sem=send_sem.at[slot],
            recv_sem=recv_sem.at[slot],
            device_id=(peer,),
            device_id_type=MESH,
        )
        made.start()
        return made

    sent = []

    def stage(copies):
        sent.extend(copies)
        return copies

    def arrive(copies):
        for made in copies:
            made.wait_recv()

    keep_z = stage([copy(features_ref, gathered.at[z, y, x, c], p) for p in z_ids])
    features = features_ref[:, :model]
    for i in (6, 7, 8):
        loads[i].wait()
    shared_hidden = (silu(dot(features, held[6][...])) * dot(features, held[7][...])).astype(
        jnp.bfloat16
    )
    shared_out = dot(shared_hidden, held[8][...])
    keep.wait()
    arrive(keep_z)
    low, high = pl.ds(0, half), pl.ds(half, nz - half)
    step = []
    view = gathered.at[low, y, x, c]
    step += [copy(view, view, p) for p in x_ids]
    view = gathered.at[high, y, x, c]
    step += [copy(view, view, p) for p in y_ids]
    arrive(stage(step))
    step = []
    view = gathered.at[low, y, :, c]
    step += [copy(view, view, p) for p in y_ids]
    view = gathered.at[high, :, x, c]
    step += [copy(view, view, p) for p in x_ids]
    arrive(stage(step))
    view = gathered.at[:, :, :, c]
    step = stage([copy(view, view, core_id)])
    for i in range(6):
        loads[i].wait()

    gate = 1.0 / (1.0 + jnp.exp(-mix_ref[...]))
    extra = width - model
    place = lax.broadcasted_iota(jnp.int32, (extra, 128), 0)
    select = jnp.where((place == me) | (place == me + experts), 1.0, 0.0).astype(jnp.bfloat16)
    rows = nz * ny * nx * seq_count

    def partial(parity):
        values = gathered[:, :, :, parity].reshape(rows, width)
        inputs = values[:, :model]
        weight = dot(values[:, model:], select)
        dense_hidden = (
            silu(dot_rows(inputs, held[0][...])) * dot_rows(inputs, held[1][...])
        ).astype(jnp.bfloat16)
        hidden = (silu(dot(inputs, held[3][...])) * dot(inputs, held[4][...])).astype(
            jnp.bfloat16
        )
        weight = jnp.concatenate([weight] * (model // 128), axis=1)
        total = gate * dot(dense_hidden, held[2][...]) + weight * dot(hidden, held[5][...])
        return total.astype(jnp.bfloat16).reshape(nz, ny, nx, seq_count, model)

    own_part[...] = partial(c)
    arrive(step)
    other_part[...] = partial(other)
    arrive(stage([copy(other_part, core_in, core_id)]))

    def add(*terms):
        total = terms[0].astype(jnp.float32)
        for term in terms[1:]:
            total = total + term.astype(jnp.float32)
        return total

    sum0[...] = add(own_part[...], core_in[...]).astype(jnp.bfloat16)
    step = []
    for d, (p, peer) in enumerate(zip(y_peers, y_ids)):
        step.append(copy(sum0.at[low, p], in1a.at[d], peer))
    for d, (p, peer) in enumerate(zip(x_peers, x_ids)):
        step.append(copy(sum0.at[high, :, p], in1b.at[d], peer))
    arrive(stage(step))
    sum1a[...] = add(sum0[low, y], *[in1a[d] for d in range(ny - 1)]).astype(jnp.bfloat16)
    sum1b[...] = add(sum0[high, :, x], *[in1b[d] for d in range(nx - 1)]).astype(jnp.bfloat16)
    step = []
    for d, (p, peer) in enumerate(zip(x_peers, x_ids)):
        step.append(copy(sum1a.at[:, p], in2a.at[d], peer))
    for d, (p, peer) in enumerate(zip(y_peers, y_ids)):
        step.append(copy(sum1b.at[:, p], in2b.at[d], peer))
    arrive(stage(step))
    sum2[low] = add(sum1a[:, x], *[in2a[d] for d in range(nx - 1)]).astype(jnp.bfloat16)
    sum2[high] = add(sum1b[:, y], *[in2b[d] for d in range(ny - 1)]).astype(jnp.bfloat16)
    step = []
    for d, (p, peer) in enumerate(zip(z_peers, z_ids)):
        step.append(copy(sum2.at[p], in3.at[d], peer))
    arrive(stage(step))
    combined = shared_out + add(sum2[z], *[in3[d] for d in range(nz - 1)])
    out_ref[...] = (residual_ref[...] + normed(combined)).astype(jnp.bfloat16)
    for made in sent:
        made.wait_send()


def ffn(features, residual, mix, weights, experts):
    dims = grid_of(lax.axis_size("ep"))
    nz, ny, nx, nc = dims
    seq_count, width = features.shape
    model = residual.shape[1]
    half = nz // 2
    rest = nz - half
    bf16 = jnp.bfloat16
    copies = 2 * (nz - 1) + 4 * (ny - 1) + 4 * (nx - 1) + 2

    def room(*shape):
        return pltpu.VMEM(tuple(max(1, s) for s in shape), bf16)

    tail = (seq_count, model)
    scratch = [pltpu.VMEM(w.shape, w.dtype) for w in weights] + [
        room(8, 128),
        room(nz, ny, nx, nc, seq_count, width),
        room(nz, ny, nx, *tail),
        room(nz, ny, nx, *tail),
        room(nz, ny, nx, *tail),
        room(nz, ny, nx, *tail),
        room(ny - 1, half, nx, *tail),
        room(nx - 1, rest, ny, *tail),
        room(half, nx, *tail),
        room(rest, ny, *tail),
        room(nx - 1, half, *tail),
        room(ny - 1, rest, *tail),
        room(nz, *tail),
        room(nz - 1, *tail),
        pltpu.SemaphoreType.DMA((10,)),
        pltpu.SemaphoreType.DMA((copies,)),
        pltpu.SemaphoreType.DMA((copies,)),
    ]
    vmem = pl.BlockSpec(memory_space=pltpu.VMEM)
    return pl.pallas_call(
        functools.partial(ffn_kernel, dims, experts),
        out_shape=jax.ShapeDtypeStruct((seq_count, model), bf16),
        in_specs=[vmem] * 3 + [pl.BlockSpec(memory_space=pl.ANY)] * len(weights),
        out_specs=vmem,
        scratch_shapes=scratch,
        compiler_params=pltpu.CompilerParams(
            collective_id=0, has_side_effects=True, vmem_limit_bytes=56 * 2**20
        ),
    )(features, residual, mix, *weights)


def per_device(
    tokens,
    lengths,
    cache_keys,
    cache_values,
    retention_state,
    mix_gain,
    query_weight,
    key_weight,
    value_weight,
    out_weight,
    ffn_gain,
    routes,
    route_scores,
    expert_gate,
    expert_up,
    expert_down,
    shared_gate,
    shared_up,
    shared_down,
    dense_gate,
    dense_up,
    dense_down,
    dense_mix,
):
    experts = lax.axis_size("ep") * expert_gate.shape[0]
    route_weight = route_scores / jnp.sum(route_scores, axis=-1, keepdims=True) * route_scale
    named = routes[:, :, None] == jnp.arange(experts, dtype=jnp.int32)[None, None, :]
    by_expert = jnp.sum(jnp.where(named, route_weight[:, :, None], 0.0), axis=1)
    coarse = lax.reduce_precision(by_expert, 8, 7)
    fine = (by_expert - coarse).astype(jnp.bfloat16)
    extra = -(-2 * experts // 128) * 128
    padding = jnp.zeros((routes.shape[0], extra - 2 * experts), jnp.bfloat16)
    residual, new_keys, new_values = retain(
        tokens,
        lengths,
        mix_gain,
        query_weight,
        key_weight,
        value_weight,
        out_weight,
        cache_keys,
        cache_values,
        retention_state,
    )
    normal_ffn = (normed(residual) * ffn_gain).astype(jnp.bfloat16)
    features = jnp.concatenate(
        [normal_ffn, coarse.astype(jnp.bfloat16), fine, padding], axis=1
    )
    weights = (
        dense_gate,
        dense_up,
        dense_down,
        expert_gate[0],
        expert_up[0],
        expert_down[0],
        shared_gate,
        shared_up,
        shared_down,
    )
    layer_out = ffn(features, residual, dense_mix[None, :], weights, experts)
    return (layer_out, new_keys, new_values)


def solution(mesh):
    in_specs = (
        P("ep", None),
        P("ep"),
        P("ep", None, None),
        P("ep", None, None),
        P("ep", None, None, None),
        P(),
        P(),
        P(),
        P(),
        P(),
        P(),
        P("ep", None),
        P("ep", None),
        P("ep", None, None),
        P("ep", None, None),
        P("ep", None, None),
        P(),
        P(),
        P(),
        P("ep", None),
        P("ep", None),
        P("ep", None),
        P(),
    )
    out_specs = (P("ep", None), P("ep", None), P("ep", None))
    return jax.shard_map(
        per_device, mesh=mesh, in_specs=in_specs, out_specs=out_specs, check_vma=False
    )
```

profile of v0, /device:TPU:0, one launch (start us, length us, event | category | flops | bytes accessed | tf_op | source)
XLA Modules:
  0.0 95.0 jit_solution(1442080215592345592)
XLA Ops:
  0.6 0.0 copy-start
  0.6 1.0 %fusion.3 = f32[16]{0:T(128)S(1)} fusion(bf16[16,1024]{1,0:T(8,128)(2,1)} %param.23), kind=kLoop, calls=%fused_computation.7 | loop fusion | flops 49136 | bytes 32832 | tf_op jit(solution)/shard_map/reduce_sum | solution.py:16
  1.7 1.6 %fusion.19 = f32[16,512]{1,0:T(8,128)S(1)} fusion(bf16[1024,512]{1,0:T(8,128)(2,1)} %param.29, bf16[16,1024]{1,0:T(8,128)(2,1)} %param.23, f32[1024]{0:T(1024)} %param.28, f32[16]{0:T(128)S(1)} %add_rsqrt_fusion.3), kind=kOutput, calls=%fused_computation.59 | convolution fusion | flops 16842752 | bytes 1118272 | tf_op jit(solution)/shard_map/dot_general | solution.py:44
  3.3 0.7 convert_element_type.79
  3.9 0.1 multiply_cosine_fusion
  4.1 0.1 multiply_subtract_fusion.1
  4.1 1.5 %fusion.17 = f32[16,512]{1,0:T(8,128)S(1)} fusion(bf16[1024,512]{1,0:T(8,128)(2,1)} %param.30, bf16[16,1024]{1,0:T(8,128)(2,1)} %param.23, f32[1024]{0:T(1024)} %param.28, f32[16]{0:T(128)S(1)} %add_rsqrt_fusion.3), kind=kOutput, calls=%fused_computation.58 | convolution fusion | flops 16842752 | bytes 1118272 | tf_op jit(solution)/shard_map/dot_general | solution.py:47
  5.7 0.1 multiply_subtract_fusion
  5.8 0.2 multiply_reduce_fusion.3
  6.0 3.9 %copy.35 = bf16[16,128,512]{1,2,0:T(8,128)(2,1)} copy(bf16[16,128,512]{2,1,0:T(8,128)(2,1)} %param.25) | data formatting | bytes 4194304 | tf_op jit(solution)/shard_map/reshape | solution.py:59
  9.9 0.0 copy-start.9
  9.9 2.2 %fusion.11 = f32[16,4,1,128]{3,2,1,0:T(1,128)S(1)} fusion(bf16[16,128,4,128]{1,3,2,0:T(8,128)(2,1)} %bitcast.37, bf16[16,4,128,1]{2,1,0,3:T(4,128)(2,1)S(1)} %bitcast.42), kind=kOutput, calls=%fused_computation.33 | convolution fusion | flops 2097152 | bytes 2146304 | tf_op jit(solution)/shard_map/shd,sjhd->shj/dot_general | solution.py:61
  12.2 0.0 copy-done.9
  12.2 0.1 maximum_convert_fusion.1
  12.3 0.1 iota_compare_fusion.1
  12.4 0.1 fusion.13
  12.5 2.8 %fusion = f32[16,4,1,256]{3,2,1,0:T(1,128)S(1)} fusion(bf16[16,16,4,8,256]{4,3,2,1,0:T(8,128)(2,1)} %bitcast.38, bf16[16,4,128,1]{2,1,0,3:T(4,128)(2,1)S(1)} %fusion.13), kind=kOutput, calls=%fused_computation | convolution fusion | flops 4194304 | bytes 4276224 | tf_op jit(solution)/shard_map/shj,sjhe->she/dot_general | solution.py:72
  15.3 0.0 copy-start.1
  15.3 0.0 copy-start.2
  15.3 0.0 copy-start.5
  15.3 6.3 %fusion.9 = f32[16,4,1,256]{3,2,1,0:T(1,128)S(1)} fusion(f32[16,4,128,256]{3,2,1,0:T(8,128)} %param.27, bf16[16,4,128,1]{2,1,0,3:T(4,128)(2,1)S(1)} %bitcast.43), kind=kOutput, calls=%fused_computation.31 | convolution fusion | flops 25165824 | bytes 8470528 | tf_op jit(solution)/shard_map/shd,shde->she/dot_general | solution.py:76
  21.6 0.0 copy-done.1
  21.6 0.0 copy-done.2
  21.6 0.0 copy-done.5
  21.6 0.0 copy-start.7
  21.6 0.0 copy-start.6
  21.6 0.0 copy-start.8
  21.7 0.4 convolution_convert_fusion
  22.1 0.0 copy-start.4
  22.1 0.1 multiply_exponential_fusion
  22.2 0.2 multiply_reduce_fusion.2
  22.4 0.1 multiply_convert_fusion.1
  22.5 0.0 copy-done
  22.5 0.5 multiply_reduce_fusion.1
  23.0 0.2 multiply_reduce_fusion
  23.2 0.0 copy-start.3
  23.3 0.0 copy-done.7
  23.3 0.1 multiply_convert_fusion
  23.3 0.0 copy-done.6
  23.4 0.0 copy-done.8
  23.4 0.1 select_reduce_fusion
  23.5 0.6 pad_maximum_fusion.features_ref
  24.1 0.0 copy-done.3
  24.1 68.9 %shard_map.238 = bf16[16,1024]{1,0:T(8,128)(2,1)} custom-call(bf16[16,1280]{1,0:T(8,128)(2,1)} %pad_maximum_fusion.features_ref, f32[16,1024]{1,0:T(8,128)} %copy-done.3, f32[1,1024]{1,0:T(1,128)} %bitcast.49, bf16[32,1024]{1,0:T(8,128)(2,1)} %refs_0_.1, bf16[32,1024]{1,0:T(8,128)(2,1)} %refs_1_.1, bf16[32,1024]{1,0:T(8,128)(2,1)} %refs_2_.1, ...), custom_call_target="tpu_custom_call" | custom-call | tf_op jit(solution)/shard_map/pallas_call | solution.py:331
  93.0 0.0 copy-done.4
  93.0 0.6 copy.54
  93.6 1.4 %copy.56 = bf16[16,1024]{1,0:T(8,128)(2,1)} copy(bf16[16,1024]{1,0:T(8,128)(2,1)} %shard_map.238) | data formatting | bytes 65536
  (15 shorter events, 0.2 us)
Async XLA Ops:
  0.6 21.9 %copy-start = (bf16[1024,1024]{1,0:T(8,128)(2,1)S(1)}, bf16[1024,1024]{1,0:T(8,128)(2,1)}, u32[]{:S(2)}) copy-start(bf16[1024,1024]{1,0:T(8,128)(2,1)} %param.32) | copy-start | bytes 6291460
  9.9 2.2 %copy-start.9 = (s32[16]{0:T(128)S(1)}, s32[16]{0:T(128)}, u32[]{:S(2)}) copy-start(s32[16]{0:T(128)} %param.24) | copy-start | bytes 196
  15.3 6.3 %copy-start.1 = (bf16[1024,1024]{1,0:T(8,128)(2,1)S(1)}, bf16[1024,1024]{1,0:T(8,128)(2,1)}, u32[]{:S(2)}) copy-start(bf16[1024,1024]{1,0:T(8,128)(2,1)} %param.31) | copy-start | bytes 6291460
  15.3 6.3 %copy-start.2 = (bf16[16,1024]{1,0:T(8,128)(2,1)S(1)}, bf16[16,1024]{1,0:T(8,128)(2,1)}, u32[]{:S(2)}) copy-start(bf16[16,1024]{1,0:T(8,128)(2,1)} %param.23) | copy-start | bytes 98308
  15.3 6.3 %copy-start.5 = (f32[1024]{0:T(1024)S(1)}, f32[1024]{0:T(1024)}, u32[]{:S(2)}) copy-start(f32[1024]{0:T(1024)} %param.28) | copy-start | bytes 12292
  21.6 1.6 %copy-start.7 = (f32[1024]{0:T(1024)S(1)}, f32[1024]{0:T(1024)}, u32[]{:S(2)}) copy-start(f32[1024]{0:T(1024)} %param.33) | copy-start | bytes 12292
  21.6 1.7 %copy-start.6 = (f32[16,6]{0,1:T(8,128)S(1)}, f32[16,6]{0,1:T(8,128)}, u32[]{:S(2)}) copy-start(f32[16,6]{0,1:T(8,128)} %param.35) | copy-start | bytes 1156
  21.6 1.7 %copy-start.8 = (s32[16,6]{0,1:T(8,128)S(1)}, s32[16,6]{0,1:T(8,128)}, u32[]{:S(2)}) copy-start(s32[16,6]{0,1:T(8,128)} %param.34) | copy-start | bytes 1156
  22.1 70.9 %copy-start.4 = (bf16[16,1024]{1,0:T(8,128)(2,1)}, bf16[16,1024]{1,0:T(8,128)(2,1)S(1)}, u32[]{:S(2)}) copy-start(bf16[16,1024]{1,0:T(8,128)(2,1)S(1)} %convolution_convert_fusion) | copy-start | bytes 98308
  23.2 0.9 copy-start.3
where the time goes:
time: 95.4 us; the launch traced here: 95 us
  Pallas kernels  68.9 us (72%)
  matrix products  15.4 us (16%)
  local copies, waits for them, and re-layouts  6.04 us (6%)
  other arithmetic  3.85 us (4%)
    pallas_call x1, Pallas kernels, ffn(): pl.pallas_call(functools.partial(ffn_kernel, dims, experts), out_shape=ja...  68.9 us
    dot_general x1, matrix products, retain(): jnp.einsum('shd,shde->she', queries.astype(jnp.float32), carry_state, pre...  6.26 us
    reshape x1, local copies, waits for them, and re-layouts, retain(): cache_keys.reshape(seq_count, block_size, head_count, key_size)  3.93 us
    dot_general x1, matrix products, retain(): jnp.einsum('shj,sjhe->she', weighted, stored_values, preferred_element_ty...  2.84 us
    dot_general x1, matrix products, retain(): jnp.einsum('shd,sjhd->shj', queries, stored_keys, preferred_element_type=...  2.24 us
    unnamed x23, local copies, waits for them, and re-layouts  2.04 us

commit v1 on v0

v1 whole, which is shorter than its diff:
```python
import functools

import jax
import jax.numpy as jnp
from jax import lax
from jax.experimental import pallas as pl
from jax.experimental.pallas import tpu as pltpu
from jax.sharding import PartitionSpec as P

eps = 1e-06
route_scale = 2.5
rope_base = 10000.0


def normed(values):
    return values * lax.rsqrt(jnp.mean(values * values, axis=-1, keepdims=True) + eps)


def log_decay(head_count):
    return jnp.log1p(-jnp.exp2(-5.0 - jnp.arange(head_count, dtype=jnp.float32)))


def rotate(values, positions):
    half_size = values.shape[-1] // 2
    inverse = rope_base ** (-jnp.arange(half_size, dtype=jnp.float32) / half_size)
    angles = positions.astype(jnp.float32)[:, None, None] * inverse[None, None, :]
    cosine = jnp.cos(angles)
    sine_part = jnp.sin(angles)
    first_half = values[..., :half_size]
    second = values[..., half_size:]
    return jnp.concatenate(
        [first_half * cosine - second * sine_part, first_half * sine_part + second * cosine],
        axis=-1,
    )


def retain(
    tokens, lengths, mix_gain, w_query, w_key, w_value, w_out, cache_keys, cache_values, carry_state
):
    seq_count, head_count, key_size, value_size = carry_state.shape
    block_size = cache_keys.shape[1]
    widened = tokens.astype(jnp.float32)
    normal_in = (normed(widened) * mix_gain).astype(jnp.bfloat16)
    raw_query = jnp.dot(normal_in, w_query, preferred_element_type=jnp.float32).reshape(
        seq_count, head_count, key_size
    )
    raw_key = jnp.dot(normal_in, w_key, preferred_element_type=jnp.float32).reshape(
        seq_count, head_count, key_size
    )
    raw_value = jnp.dot(normal_in, w_value, preferred_element_type=jnp.float32).reshape(
        seq_count, head_count, value_size
    )
    queries = (rotate(raw_query, lengths) * key_size ** (-0.5)).astype(jnp.bfloat16)
    new_keys = rotate(raw_key, lengths).astype(jnp.bfloat16)
    new_values = raw_value.astype(jnp.bfloat16)
    filled = lengths % block_size
    decay_rate = log_decay(head_count)
    places = jnp.arange(block_size, dtype=jnp.int32)
    stored_keys = cache_keys.reshape(seq_count, block_size, head_count, key_size)
    stored_values = cache_values.reshape(seq_count, block_size, head_count, value_size)
    scores = jnp.einsum("shd,sjhd->shj", queries, stored_keys, preferred_element_type=jnp.float32)
    distance = jnp.maximum(filled[:, None] - places[None, :], 0).astype(jnp.float32)
    live_mask = places[None, :] < filled[:, None]
    weighted = jnp.where(
        live_mask[:, None, :],
        scores * jnp.exp(distance[:, None, :] * decay_rate[None, :, None]),
        0.0,
    ).astype(jnp.bfloat16)
    own_weight = jnp.sum(
        queries.astype(jnp.float32) * new_keys.astype(jnp.float32), axis=-1
    ).astype(jnp.bfloat16)
    inside = jnp.einsum(
        "shj,sjhe->she", weighted, stored_values, preferred_element_type=jnp.float32
    )
    inside = inside + own_weight.astype(jnp.float32)[:, :, None] * new_values.astype(jnp.float32)
    carried = jnp.einsum(
        "shd,shde->she", queries.astype(jnp.float32), carry_state, precision=lax.Precision.HIGHEST
    )
    carried = (
        carried
        * jnp.exp((filled.astype(jnp.float32)[:, None] + 1.0) * decay_rate[None, :])[:, :, None]
    )
    headed = (
        normed(inside + carried).astype(jnp.bfloat16).reshape(seq_count, head_count * value_size)
    )
    mixer_out = jnp.dot(headed, w_out, preferred_element_type=jnp.float32)
    residual = widened + normed(mixer_out)
    return (
        residual,
        new_keys.reshape(seq_count, head_count * key_size),
        new_values.reshape(seq_count, head_count * value_size),
    )


MESH = pl.DeviceIdType.MESH


def grid_of(count):
    cores = 2 if count % 2 == 0 else 1
    chips = count // cores
    x_size = max(d for d in range(1, chips + 1) if chips % d == 0 and d**3 <= chips)
    plane = chips // x_size
    y_size = max(d for d in range(1, plane + 1) if plane % d == 0 and d**2 <= plane)
    return plane // y_size, y_size, x_size, cores


def silu(values):
    return values * (1.0 / (1.0 + jnp.exp(-values)))


def dot(left, right):
    return jnp.dot(left, right, preferred_element_type=jnp.float32)


def dot_rows(left, right):
    return lax.dot_general(
        left, right, (((1,), (1,)), ((), ())), preferred_element_type=jnp.float32
    )


def slot_tables(routes, scores, experts):
    seq_count, top = routes.shape
    bf16 = jnp.bfloat16
    weight = scores / jnp.sum(scores, axis=-1, keepdims=True) * route_scale
    lanes = lax.broadcasted_iota(jnp.int32, (seq_count, experts), 1)
    member = jnp.zeros((seq_count, experts), jnp.float32)
    by_expert = jnp.zeros((seq_count, experts), jnp.float32)
    for k in range(top):
        named = routes[:, k : k + 1] == lanes
        member = jnp.where(named, 1.0, member)
        by_expert = jnp.where(named, weight[:, k : k + 1], by_expert)
    row = lax.broadcasted_iota(jnp.int32, (seq_count, seq_count), 0)
    column = lax.broadcasted_iota(jnp.int32, (seq_count, seq_count), 1)
    before = jnp.where(column < row, 1.0, 0.0).astype(bf16)
    rank = dot(before, member.astype(bf16))
    first = jnp.where(rank < 0.5, member, 0.0)
    second = member - first
    source = lax.broadcasted_iota(jnp.int32, (experts, 2 * experts), 0)
    slot = lax.broadcasted_iota(jnp.int32, (experts, 2 * experts), 1)
    to_first = jnp.where(slot == 2 * source, 1.0, 0.0).astype(bf16)
    to_second = jnp.where(slot == 2 * source + 1, 1.0, 0.0).astype(bf16)

    def spread(values):
        return dot((first * values).astype(bf16), to_first) + dot(
            (second * values).astype(bf16), to_second
        )

    coarse = by_expert.astype(bf16).astype(jnp.float32)
    fine = by_expert - coarse
    pick = spread(jnp.ones_like(by_expert))
    return pick.T.astype(bf16), spread(coarse).astype(bf16), spread(fine).astype(bf16)


def ffn_kernel(
    dims,
    features_ref,
    residual_ref,
    routes_ref,
    scores_ref,
    mix_ref,
    dense_gate_ref,
    dense_up_ref,
    dense_down_ref,
    expert_gate_ref,
    expert_up_ref,
    expert_down_ref,
    shared_gate_ref,
    shared_up_ref,
    shared_down_ref,
    out_ref,
    expert_gate,
    expert_up,
    expert_down,
    shared_gate,
    shared_up,
    shared_down,
    dense_weights,
    rows_out,
    rows_in,
    answers_out,
    answers_in,
    measure,
    group_tokens,
    group_part,
    in_1a,
    in_1b,
    sum_1a,
    sum_1b,
    in_2a,
    in_2b,
    local_sem,
    link_send,
    link_recv,
    row_send,
    row_recv,
):
    nz, ny, nx, nc = dims
    count = nz * ny * nx * nc
    seq_count, model = features_ref.shape
    part = model // 2
    bf16 = jnp.bfloat16
    me = lax.axis_index("ep")
    c = lax.rem(me, nc)
    x = lax.rem(me // nc, nx)
    y = lax.rem(me // (nc * nx), ny)
    z = me // (nc * nx * ny)

    def at(z_at, y_at, x_at, c_at):
        return ((z_at * ny + y_at) * nx + x_at) * nc + c_at

    barrier = pltpu.get_barrier_semaphore()

    def greet(i, carry):
        pl.semaphore_signal(
            barrier, inc=1, device_id=(lax.rem(me + i, count),), device_id_type=MESH
        )
        return carry

    lax.fori_loop(1, count, greet, 0)

    loads = [
        pltpu.make_async_copy(dense_gate_ref, dense_weights.at[0, z, c], local_sem.at[0]),
        pltpu.make_async_copy(dense_up_ref, dense_weights.at[1, z, c], local_sem.at[1]),
        pltpu.make_async_copy(dense_down_ref, dense_weights.at[2, z, c], local_sem.at[2]),
        pltpu.make_async_copy(shared_gate_ref, shared_gate, local_sem.at[3]),
        pltpu.make_async_copy(shared_up_ref, shared_up, local_sem.at[4]),
        pltpu.make_async_copy(shared_down_ref, shared_down, local_sem.at[5]),
        pltpu.make_async_copy(expert_gate_ref.at[0], expert_gate, local_sem.at[6]),
        pltpu.make_async_copy(expert_up_ref.at[0], expert_up, local_sem.at[7]),
        pltpu.make_async_copy(expert_down_ref.at[0], expert_down, local_sem.at[8]),
    ]
    for load in loads:
        load.start()

    y_peers = [lax.rem(y + d, ny) for d in range(1, ny)]
    x_peers = [lax.rem(x + d, nx) for d in range(1, nx)]
    z_ids = [at(lax.rem(z + d, nz), y, x, c) for d in range(1, nz)]
    y_ids = [at(z, p, x, c) for p in y_peers]
    x_ids = [at(z, y, p, c) for p in x_peers]
    core_id = at(z, y, x, nc - 1 - c)

    slots = iter(range(1000))
    sent = []

    def copy(src, dst, peer):
        slot = next(slots)
        made = pltpu.make_async_remote_copy(
            src_ref=src,
            dst_ref=dst,
            send_sem=link_send.at[slot],
            recv_sem=link_recv.at[slot],
            device_id=(peer,),
            device_id_type=MESH,
        )
        made.start()
        sent.append(made)
        return made

    def arrive(copies):
        for made in copies:
            made.wait_recv()

    def pair_of(ref, device):
        return ref.at[pl.ds(pl.multiple_of(2 * device, 2), 2), :]

    def exchange(source, target, phase):
        def send(i, carry):
            peer = lax.rem(me + i, count)
            pltpu.make_async_remote_copy(
                src_ref=pair_of(source, peer),
                dst_ref=pair_of(target, me),
                send_sem=row_send.at[phase],
                recv_sem=row_recv.at[phase],
                device_id=(peer,),
                device_id_type=MESH,
            ).start()
            return carry

        lax.fori_loop(1, count, send, 0)

    def everything(phase):
        return pltpu.make_async_remote_copy(
            src_ref=measure,
            dst_ref=measure,
            send_sem=row_send.at[phase],
            recv_sem=row_recv.at[phase],
            device_id=(core_id,),
            device_id_type=MESH,
        )

    row = lax.broadcasted_iota(jnp.int32, rows_in.shape, 0)
    mine = (row >= 2 * me) & (row < 2 * me + 2)

    def completed(own, received):
        return jnp.where(mine, own[...].astype(jnp.float32), received[...].astype(jnp.float32))

    pick, coarse, fine = slot_tables(routes_ref[...], scores_ref[...], count)
    features = features_ref[...]
    group_tokens[y, x] = features
    rows_out[...] = dot(pick, features).astype(bf16)
    for load in loads[:3]:
        load.wait()

    pl.semaphore_wait(barrier, count - 1)

    first, last = pl.ds(0, part), pl.ds(part, part)
    gather_1a = []
    gather_1b = []
    view = group_tokens.at[y, x, :, first]
    gather_1a += [copy(view, view, p) for p in x_ids]
    view = group_tokens.at[y, x, :, last]
    gather_1b += [copy(view, view, p) for p in y_ids]
    exchange(rows_out, rows_in, 0)
    view = dense_weights.at[:, z, c]
    from_z = [copy(view, view, p) for p in z_ids]
    for load in loads[3:6]:
        load.wait()
    shared_hidden = (silu(dot(features, shared_gate[...])) * dot(features, shared_up[...])).astype(
        bf16
    )
    shared_out = dot(shared_hidden, shared_down[...])
    arrive(gather_1a)
    view = group_tokens.at[y, :, :, first]
    gather_2 = [copy(view, view, p) for p in y_ids]
    arrive(gather_1b)
    view = group_tokens.at[:, x, :, last]
    gather_2 += [copy(view, view, p) for p in x_ids]
    arrive(from_z)
    view = dense_weights.at[:, :, c]
    from_core = [copy(view, view, core_id)]

    for load in loads[6:]:
        load.wait()
    everything(0).wait_recv()
    inputs = completed(rows_out, rows_in).astype(bf16)
    hidden = (silu(dot(inputs, expert_gate[...])) * dot(inputs, expert_up[...])).astype(bf16)
    answers_out[...] = dot(hidden, expert_down[...]).astype(bf16)
    exchange(answers_out, answers_in, 1)

    arrive(gather_2)
    arrive(from_core)
    units = nz * nc * dense_gate_ref.shape[0]
    inputs = group_tokens[...].reshape(ny * nx * seq_count, model)
    hidden = (
        silu(dot_rows(inputs, dense_weights[0].reshape(units, model)))
        * dot_rows(inputs, dense_weights[1].reshape(units, model))
    ).astype(bf16)
    group_part[...] = (
        dot(hidden, dense_weights[2].reshape(units, model))
        .astype(bf16)
        .reshape(ny, nx, seq_count, model)
    )
    step = []
    for d, (p, peer) in enumerate(zip(y_peers, y_ids)):
        step.append(copy(group_part.at[p, :, :, first], in_1a.at[d], peer))
    for d, (p, peer) in enumerate(zip(x_peers, x_ids)):
        step.append(copy(group_part.at[:, p, :, last], in_1b.at[d], peer))

    def add(*terms):
        total = terms[0].astype(jnp.float32)
        for term in terms[1:]:
            total = total + term.astype(jnp.float32)
        return total

    arrive(step)
    sum_1a[...] = add(group_part[y, :, :, :part], *[in_1a[d] for d in range(ny - 1)]).astype(bf16)
    sum_1b[...] = add(group_part[:, x, :, part:], *[in_1b[d] for d in range(nx - 1)]).astype(bf16)
    step = []
    for d, (p, peer) in enumerate(zip(x_peers, x_ids)):
        step.append(copy(sum_1a.at[p], in_2a.at[d], peer))
    for d, (p, peer) in enumerate(zip(y_peers, y_ids)):
        step.append(copy(sum_1b.at[p], in_2b.at[d], peer))
    arrive(step)
    dense_out = jnp.concatenate(
        [
            add(sum_1a[x], *[in_2a[d] for d in range(nx - 1)]),
            add(sum_1b[y], *[in_2b[d] for d in range(ny - 1)]),
        ],
        axis=-1,
    )
    gate = 1.0 / (1.0 + jnp.exp(-mix_ref[...]))
    combined = shared_out + gate * dense_out

    everything(1).wait_recv()
    answers = completed(answers_out, answers_in).astype(bf16)
    combined = combined + (dot(coarse, answers) + dot(fine, answers))
    out_ref[...] = (residual_ref[...] + normed(combined)).astype(bf16)
    for made in sent + [everything(0), everything(1)]:
        made.wait_send()


def ffn(features, residual, routes, scores, mix, weights):
    dims = grid_of(lax.axis_size("ep"))
    nz, ny, nx, nc = dims
    count = lax.axis_size("ep")
    seq_count, model = features.shape
    part = model // 2
    bf16 = jnp.bfloat16
    dense_gate, expert_gate, expert_down, shared_gate, shared_down = (
        weights[0],
        weights[3],
        weights[5],
        weights[6],
        weights[8],
    )
    copies = 4 * (ny - 1) + 4 * (nx - 1) + (nz - 1) + 1

    def room(*shape):
        return pltpu.VMEM(shape, bf16)

    rows = (2 * count, model)
    scratch = [
        room(*expert_gate.shape[1:]),
        room(*expert_gate.shape[1:]),
        room(*expert_down.shape[1:]),
        room(*shared_gate.shape),
        room(*shared_gate.shape),
        room(*shared_down.shape),
        room(3, nz, nc, *dense_gate.shape),
        room(*rows),
        room(*rows),
        room(*rows),
        room(*rows),
        room(2 * (count - 1) * model // 256, 256),
        room(ny, nx, seq_count, model),
        room(ny, nx, seq_count, model),
        room(ny - 1, nx, seq_count, part),
        room(nx - 1, ny, seq_count, part),
        room(nx, seq_count, part),
        room(ny, seq_count, part),
        room(nx - 1, seq_count, part),
        room(ny - 1, seq_count, part),
        pltpu.SemaphoreType.DMA((9,)),
        pltpu.SemaphoreType.DMA((copies,)),
        pltpu.SemaphoreType.DMA((copies,)),
        pltpu.SemaphoreType.DMA((2,)),
        pltpu.SemaphoreType.DMA((2,)),
    ]
    vmem = pl.BlockSpec(memory_space=pltpu.VMEM)
    return pl.pallas_call(
        functools.partial(ffn_kernel, dims),
        out_shape=jax.ShapeDtypeStruct((seq_count, model), bf16),
        in_specs=[vmem] * 5 + [pl.BlockSpec(memory_space=pl.ANY)] * len(weights),
        out_specs=vmem,
        scratch_shapes=scratch,
        compiler_params=pltpu.CompilerParams(
            collective_id=0, has_side_effects=True, vmem_limit_bytes=56 * 2**20
        ),
    )(features, residual, routes, scores, mix, *weights)


def per_device(
    tokens,
    lengths,
    cache_keys,
    cache_values,
    retention_state,
    mix_gain,
    query_weight,
    key_weight,
    value_weight,
    out_weight,
    ffn_gain,
    routes,
    route_scores,
    expert_gate,
    expert_up,
    expert_down,
    shared_gate,
    shared_up,
    shared_down,
    dense_gate,
    dense_up,
    dense_down,
    dense_mix,
):
    residual, new_keys, new_values = retain(
        tokens,
        lengths,
        mix_gain,
        query_weight,
        key_weight,
        value_weight,
        out_weight,
        cache_keys,
        cache_values,
        retention_state,
    )
    features = (normed(residual) * ffn_gain).astype(jnp.bfloat16)
    weights = (
        dense_gate,
        dense_up,
        dense_down,
        expert_gate,
        expert_up,
        expert_down,
        shared_gate,
        shared_up,
        shared_down,
    )
    layer_out = ffn(features, residual, routes, route_scores, dense_mix[None, :], weights)
    return (layer_out, new_keys, new_values)


def solution(mesh):
    in_specs = (
        P("ep", None),
        P("ep"),
        P("ep", None, None),
        P("ep", None, None),
        P("ep", None, None, None),
        P(),
        P(),
        P(),
        P(),
        P(),
        P(),
        P("ep", None),
        P("ep", None),
        P("ep", None, None),
        P("ep", None, None),
        P("ep", None, None),
        P(),
        P(),
        P(),
        P("ep", None),
        P("ep", None),
        P("ep", None),
        P(),
    )
    out_specs = (P("ep", None), P("ep", None), P("ep", None))
    return jax.shard_map(
        per_device, mesh=mesh, in_specs=in_specs, out_specs=out_specs, check_vma=False
    )
```

time: 95.4 us -> 73.3 us (0.77)
  Pallas kernels: 68.9 us -> 45.6 us
  local copies, waits for them, and re-layouts: 6.04 us -> 7.37 us
    pallas_call x1, Pallas kernels: 68.9 us -> 45.6 us  [ffn(): pl.pallas_call(functools.partial(ffn_kernel, dims), out_shape=jax.ShapeDt...]
    unnamed x23 -> x25, local copies, waits for them, and re-layouts: 2.04 us -> 3.4 us
where the time goes in v1:
time: 73.3 us; the launch traced here: 72.9 us
  Pallas kernels  45.6 us (62%)
  matrix products  15.4 us (21%)
  local copies, waits for them, and re-layouts  7.37 us (10%)
  other arithmetic  3.73 us (5%)
  between operations  0.83 us (1%)
    pallas_call x1, Pallas kernels, ffn(): pl.pallas_call(functools.partial(ffn_kernel, dims), out_shape=jax.ShapeDt...  45.6 us
    dot_general x1, matrix products, retain(): jnp.einsum('shd,shde->she', queries.astype(jnp.float32), carry_state, pre...  6.26 us
    reshape x1, local copies, waits for them, and re-layouts, retain(): cache_keys.reshape(seq_count, block_size, head_count, key_size)  3.91 us
    unnamed x25, local copies, waits for them, and re-layouts  3.4 us
    dot_general x1, matrix products, retain(): jnp.einsum('shj,sjhe->she', weighted, stored_values, preferred_element_ty...  2.84 us
    dot_general x1, matrix products, retain(): jnp.einsum('shd,sjhd->shj', queries, stored_keys, preferred_element_type=...  2.24 us
    dot_general x1, matrix products, retain(): jnp.dot(normal_in, w_query, preferred_element_type=jnp.float32)  1.55 us
    dot_general x1, matrix products, retain(): jnp.dot(normal_in, w_key, preferred_element_type=jnp.float32)  1.55 us

profile of v1, /device:TPU:0, one launch (start us, length us, event | category | flops | bytes accessed | tf_op | source)
XLA Modules:
  0.0 72.9 jit_solution(10351175638237608476)
XLA Ops:
  0.6 0.0 copy-start
  0.6 1.0 %fusion.3 = f32[16]{0:T(128)S(1)} fusion(bf16[16,1024]{1,0:T(8,128)(2,1)} %param.23), kind=kLoop, calls=%fused_computation.7 | loop fusion | flops 49136 | bytes 32832 | tf_op jit(solution)/shard_map/reduce_sum | solution.py:16
  1.7 1.6 %fusion.18 = f32[16,512]{1,0:T(8,128)S(1)} fusion(bf16[1024,512]{1,0:T(8,128)(2,1)} %param.29, bf16[16,1024]{1,0:T(8,128)(2,1)} %param.23, f32[1024]{0:T(1024)} %param.28, f32[16]{0:T(128)S(1)} %add_rsqrt_fusion.3), kind=kOutput, calls=%fused_computation.52 | convolution fusion | flops 16842752 | bytes 1118272 | tf_op jit(solution)/shard_map/dot_general | solution.py:44
  3.3 0.7 convert_element_type.73
  3.9 0.1 multiply_cosine_fusion
  4.1 0.1 multiply_subtract_fusion.1
  4.1 1.5 %fusion.16 = f32[16,512]{1,0:T(8,128)S(1)} fusion(bf16[1024,512]{1,0:T(8,128)(2,1)} %param.30, bf16[16,1024]{1,0:T(8,128)(2,1)} %param.23, f32[1024]{0:T(1024)} %param.28, f32[16]{0:T(128)S(1)} %add_rsqrt_fusion.3), kind=kOutput, calls=%fused_computation.51 | convolution fusion | flops 16842752 | bytes 1118272 | tf_op jit(solution)/shard_map/dot_general | solution.py:47
  5.7 0.1 multiply_subtract_fusion
  5.8 0.2 multiply_reduce_fusion.3
  6.0 3.9 %copy.35 = bf16[16,128,512]{1,2,0:T(8,128)(2,1)} copy(bf16[16,128,512]{2,1,0:T(8,128)(2,1)} %param.25) | data formatting | bytes 4194304 | tf_op jit(solution)/shard_map/reshape | solution.py:59
  9.9 0.0 copy-start.9
  9.9 2.2 %fusion.11 = f32[16,4,1,128]{3,2,1,0:T(1,128)S(1)} fusion(bf16[16,128,4,128]{1,3,2,0:T(8,128)(2,1)} %bitcast.34, bf16[16,4,128,1]{2,1,0,3:T(4,128)(2,1)S(1)} %bitcast.36), kind=kOutput, calls=%fused_computation.30 | convolution fusion | flops 2097152 | bytes 2146304 | tf_op jit(solution)/shard_map/shd,sjhd->shj/dot_general | solution.py:61
  12.2 0.0 copy-done.9
  12.2 0.1 maximum_convert_fusion.1
  12.3 0.1 iota_compare_fusion
  12.4 0.1 fusion.13
  12.5 2.8 %fusion = f32[16,4,1,256]{3,2,1,0:T(1,128)S(1)} fusion(bf16[16,16,4,8,256]{4,3,2,1,0:T(8,128)(2,1)} %bitcast.35, bf16[16,4,128,1]{2,1,0,3:T(4,128)(2,1)S(1)} %fusion.13), kind=kOutput, calls=%fused_computation | convolution fusion | flops 4194304 | bytes 4276224 | tf_op jit(solution)/shard_map/shj,sjhe->she/dot_general | solution.py:72
  15.3 0.0 copy-start.1
  15.3 0.0 copy-start.2
  15.3 0.0 copy-start.5
  15.3 6.3 %fusion.9 = f32[16,4,1,256]{3,2,1,0:T(1,128)S(1)} fusion(f32[16,4,128,256]{3,2,1,0:T(8,128)} %param.27, bf16[16,4,128,1]{2,1,0,3:T(4,128)(2,1)S(1)} %bitcast.37), kind=kOutput, calls=%fused_computation.28 | convolution fusion | flops 25165824 | bytes 8470528 | tf_op jit(solution)/shard_map/shd,shde->she/dot_general | solution.py:76
  21.6 0.0 copy-done.1
  21.6 0.0 copy-done.2
  21.6 0.0 copy-done.5
  21.6 0.0 copy-start.6
  21.6 0.0 copy-start.7
  21.6 0.0 copy-start.8
  21.6 0.4 convolution_convert_fusion
  22.1 0.0 copy-start.4
  22.1 0.1 multiply_exponential_fusion
  22.2 0.2 multiply_reduce_fusion.2
  22.4 0.1 multiply_convert_fusion.1
  22.5 0.0 copy-done
  22.5 0.5 multiply_reduce_fusion.1
  23.0 0.2 multiply_reduce_fusion
  23.2 0.0 copy-start.3
  23.2 0.0 copy-done.6
  23.2 0.7 multiply_convert_fusion.features_ref
  23.9 0.0 copy-done.7
  23.9 0.7 copy.26.routes_ref
  24.6 0.0 copy-done.8
  24.6 0.7 copy.27.scores_ref
  25.3 0.0 copy-done.3
  25.3 45.6 %shard_map.238 = bf16[16,1024]{1,0:T(8,128)(2,1)} custom-call(bf16[16,1024]{1,0:T(8,128)(2,1)} %multiply_convert_fusion.features_ref, f32[16,1024]{1,0:T(8,128)} %copy-done.3, s32[16,6]{1,0:T(8,128)} %copy.26.routes_ref, f32[16,6]{1,0:T(8,128)} %copy.27.scores_ref, f32[1,1024]{1,0:T(1,128)} %bitcast.43, bf16[32,1024]{1,0:T(8,128)(2,1)} %dense_gate_ref.1, ...), custom_call_target="tpu_custom_call" | custom-call | tf_op jit(solution)/shard_map/pallas_call | solution.py:440
  70.9 0.0 copy-done.4
  70.9 0.6 copy.54
  71.5 1.4 %copy.56 = bf16[16,1024]{1,0:T(8,128)(2,1)} copy(bf16[16,1024]{1,0:T(8,128)(2,1)} %shard_map.238) | data formatting | bytes 65536
  (12 shorter events, 0.2 us)
Async XLA Ops:
  0.6 21.9 %copy-start = (bf16[1024,1024]{1,0:T(8,128)(2,1)S(1)}, bf16[1024,1024]{1,0:T(8,128)(2,1)}, u32[]{:S(2)}) copy-start(bf16[1024,1024]{1,0:T(8,128)(2,1)} %param.32) | copy-start | bytes 6291460
  9.9 2.2 %copy-start.9 = (s32[16]{0:T(128)S(1)}, s32[16]{0:T(128)}, u32[]{:S(2)}) copy-start(s32[16]{0:T(128)} %param.24) | copy-start | bytes 196
  15.3 6.3 %copy-start.1 = (bf16[1024,1024]{1,0:T(8,128)(2,1)S(1)}, bf16[1024,1024]{1,0:T(8,128)(2,1)}, u32[]{:S(2)}) copy-start(bf16[1024,1024]{1,0:T(8,128)(2,1)} %param.31) | copy-start | bytes 6291460
  15.3 6.3 %copy-start.2 = (bf16[16,1024]{1,0:T(8,128)(2,1)S(1)}, bf16[16,1024]{1,0:T(8,128)(2,1)}, u32[]{:S(2)}) copy-start(bf16[16,1024]{1,0:T(8,128)(2,1)} %param.23) | copy-start | bytes 98308
  15.3 6.3 %copy-start.5 = (f32[1024]{0:T(1024)S(1)}, f32[1024]{0:T(1024)}, u32[]{:S(2)}) copy-start(f32[1024]{0:T(1024)} %param.28) | copy-start | bytes 12292
  21.6 1.6 %copy-start.6 = (f32[1024]{0:T(1024)S(1)}, f32[1024]{0:T(1024)}, u32[]{:S(2)}) copy-start(f32[1024]{0:T(1024)} %param.33) | copy-start | bytes 12292
  21.6 2.3 %copy-start.7 = (s32[16,6]{0,1:T(8,128)S(1)}, s32[16,6]{0,1:T(8,128)}, u32[]{:S(2)}) copy-start(s32[16,6]{0,1:T(8,128)} %param.34) | copy-start | bytes 1156
  21.6 3.0 %copy-start.8 = (f32[16,6]{0,1:T(8,128)S(1)}, f32[16,6]{0,1:T(8,128)}, u32[]{:S(2)}) copy-start(f32[16,6]{0,1:T(8,128)} %param.35) | copy-start | bytes 1156
  22.1 48.9 %copy-start.4 = (bf16[16,1024]{1,0:T(8,128)(2,1)}, bf16[16,1024]{1,0:T(8,128)(2,1)S(1)}, u32[]{:S(2)}) copy-start(bf16[16,1024]{1,0:T(8,128)(2,1)S(1)} %convolution_convert_fusion) | copy-start | bytes 98308
  23.2 2.1 %copy-start.3 = (f32[16,1024]{1,0:T(8,128)}, f32[16,1024]{1,0:T(8,128)S(1)}, u32[]{:S(2)}) copy-start(f32[16,1024]{1,0:T(8,128)S(1)} %get-tuple-element.4.residual_ref) | copy-start | bytes 196612

commit v2 on v1

v2 whole, which is shorter than its diff:
```python
import functools
import math

import jax
import jax.numpy as jnp
from jax import lax
from jax.experimental import pallas as pl
from jax.experimental.pallas import tpu as pltpu
from jax.sharding import PartitionSpec as P

eps = 1e-06
route_scale = 2.5
rope_base = 10000.0


def normed(values):
    return values * lax.rsqrt(jnp.mean(values * values, axis=-1, keepdims=True) + eps)


MESH = pl.DeviceIdType.MESH


def grid_of(count):
    cores = 2 if count % 2 == 0 else 1
    chips = count // cores
    x_size = max(d for d in range(1, chips + 1) if chips % d == 0 and d**3 <= chips)
    plane = chips // x_size
    y_size = max(d for d in range(1, plane + 1) if plane % d == 0 and d**2 <= plane)
    return plane // y_size, y_size, x_size, cores


def silu(values):
    return values * (1.0 / (1.0 + jnp.exp(-values)))


def dot(left, right):
    return jnp.dot(left, right, preferred_element_type=jnp.float32)


def dot_rows(left, right):
    return lax.dot_general(
        left, right, (((1,), (1,)), ((), ())), preferred_element_type=jnp.float32
    )


def slot_tables(routes, scores, experts):
    top, seq_count = routes.shape
    bf16 = jnp.bfloat16
    weight = scores / jnp.sum(scores, axis=0, keepdims=True) * route_scale
    expert = lax.broadcasted_iota(jnp.int32, (experts, seq_count), 0)
    member = jnp.zeros((experts, seq_count), jnp.float32)
    by_expert = jnp.zeros((experts, seq_count), jnp.float32)
    for k in range(top):
        named = routes[k : k + 1, :] == expert
        member = jnp.where(named, 1.0, member)
        by_expert = jnp.where(named, weight[k : k + 1, :], by_expert)
    row = lax.broadcasted_iota(jnp.int32, (seq_count, seq_count), 0)
    column = lax.broadcasted_iota(jnp.int32, (seq_count, seq_count), 1)
    before = jnp.where(row < column, 1.0, 0.0).astype(bf16)
    rank = dot(member.astype(bf16), before)
    first = jnp.where(rank < 0.5, member, 0.0)
    second = member - first
    slot = lax.broadcasted_iota(jnp.int32, (2 * experts, experts), 0)
    source = lax.broadcasted_iota(jnp.int32, (2 * experts, experts), 1)
    to_first = jnp.where(slot == 2 * source, 1.0, 0.0).astype(bf16)
    to_second = jnp.where(slot == 2 * source + 1, 1.0, 0.0).astype(bf16)

    def spread(values):
        return dot(to_first, (first * values).astype(bf16)) + dot(
            to_second, (second * values).astype(bf16)
        )

    coarse = by_expert.astype(bf16).astype(jnp.float32)
    fine = by_expert - coarse
    pick = spread(jnp.ones_like(by_expert)).astype(bf16)
    return pick, spread(coarse).T.astype(bf16), spread(fine).T.astype(bf16)


def layer_kernel(
    dims,
    lengths_ref,
    tokens_hbm,
    cache_keys_hbm,
    cache_values_hbm,
    state_hbm,
    mix_gain_hbm,
    query_weight_hbm,
    key_weight_hbm,
    value_weight_hbm,
    out_weight_hbm,
    ffn_gain_hbm,
    routes_hbm,
    scores_hbm,
    expert_gate_hbm,
    expert_up_hbm,
    expert_down_hbm,
    shared_gate_hbm,
    shared_up_hbm,
    shared_down_hbm,
    dense_gate_hbm,
    dense_up_hbm,
    dense_down_hbm,
    mix_hbm,
    out_ref,
    new_keys_ref,
    new_values_ref,
    tokens,
    cache_keys,
    cache_values,
    state,
    mix_gain,
    query_weight,
    key_weight,
    value_weight,
    out_weight,
    ffn_gain,
    routes,
    scores,
    mix,
    expert_gate,
    expert_up,
    expert_down,
    shared_gate,
    shared_up,
    shared_down,
    dense_weights,
    queries,
    turned,
    block_scores,
    inside,
    carried,
    rows_out,
    rows_in,
    answers_out,
    answers_in,
    measure,
    group_tokens,
    group_part,
    in_1a,
    in_1b,
    sum_1a,
    sum_1b,
    in_2a,
    in_2b,
    local_sem,
    link_send,
    link_recv,
    row_send,
    row_recv,
    entry_sem,
):
    nz, ny, nx, nc = dims
    count = nz * ny * nx * nc
    seq_count, model = tokens.shape
    heads, key_size, value_size = state.shape[1:]
    block = cache_keys.shape[1]
    part = model // 2
    bf16 = jnp.bfloat16
    f32 = jnp.float32
    me = lax.axis_index("ep")
    c = lax.rem(me, nc)
    x = lax.rem(me // nc, nx)
    y = lax.rem(me // (nc * nx), ny)
    z = me // (nc * nx * ny)

    def at(z_at, y_at, x_at, c_at):
        return ((z_at * ny + y_at) * nx + x_at) * nc + c_at

    local_slots = iter(range(1000))

    def load(source, target):
        made = pltpu.make_async_copy(source, target, local_sem.at[next(local_slots)])
        made.start()
        return made

    def ready(loads):
        for made in loads:
            made.wait()

    chunk = seq_count // 4
    chunks = [pl.ds(i, chunk) for i in range(0, seq_count, chunk)]
    dense_loads = [
        load(dense_gate_hbm, dense_weights.at[0, z, c]),
        load(dense_up_hbm, dense_weights.at[1, z, c]),
        load(dense_down_hbm, dense_weights.at[2, z, c]),
    ]
    first_loads = [
        load(tokens_hbm, tokens),
        load(mix_gain_hbm, mix_gain),
        load(query_weight_hbm, query_weight),
        load(key_weight_hbm, key_weight),
    ]
    route_loads = [load(routes_hbm, routes), load(scores_hbm, scores)]
    key_loads = [load(cache_keys_hbm.at[s], cache_keys.at[s]) for s in chunks]
    value_loads = [load(value_weight_hbm, value_weight)]

    barrier = pltpu.get_barrier_semaphore()

    y_peers = [lax.rem(y + d, ny) for d in range(1, ny)]
    x_peers = [lax.rem(x + d, nx) for d in range(1, nx)]
    z_ids = [at(lax.rem(z + d, nz), y, x, c) for d in range(1, nz)]
    y_ids = [at(z, p, x, c) for p in y_peers]
    x_ids = [at(z, y, p, c) for p in x_peers]
    core_id = at(z, y, x, nc - 1 - c)

    across = [at(z, y, p, nc - 1 - c) for p in x_peers]
    lines = x_ids + across + [core_id] + y_ids + z_ids
    for peer in lines:
        pl.semaphore_signal(barrier, inc=1, device_id=(peer,), device_id_type=MESH)

    def spread_entry(semaphore, peers):
        for peer in peers:
            pl.semaphore_signal(semaphore, inc=1, device_id=(peer,), device_id_type=MESH)

    slots = iter(range(1000))
    sent = []

    def copy(src, dst, peer):
        slot = next(slots)
        made = pltpu.make_async_remote_copy(
            src_ref=src,
            dst_ref=dst,
            send_sem=link_send.at[slot],
            recv_sem=link_recv.at[slot],
            device_id=(peer,),
            device_id_type=MESH,
        )
        made.start()
        sent.append(made)
        return made

    def arrive(copies):
        for made in copies:
            made.wait_recv()

    def pair_of(ref, device):
        return ref.at[pl.ds(pl.multiple_of(2 * device, 2), 2), :]

    def exchange(source, target, phase):
        def send(i, carry):
            peer = lax.rem(me + i, count)
            pltpu.make_async_remote_copy(
                src_ref=pair_of(source, peer),
                dst_ref=pair_of(target, me),
                send_sem=row_send.at[phase],
                recv_sem=row_recv.at[phase],
                device_id=(peer,),
                device_id_type=MESH,
            ).start()
            return carry

        lax.fori_loop(1, count, send, 0)

    def everything(phase):
        return pltpu.make_async_remote_copy(
            src_ref=measure,
            dst_ref=measure,
            send_sem=row_send.at[phase],
            recv_sem=row_recv.at[phase],
            device_id=(core_id,),
            device_id_type=MESH,
        )

    near = pl.ds(pl.multiple_of(me // 8 * 16, 16), 16)
    near_row = lax.broadcasted_iota(jnp.int32, (16, model), 0)
    own_row = 2 * lax.rem(me, 8)
    mine = (near_row >= own_row) & (near_row < own_row + 2)

    def complete(own, received):
        received[near, :] = jnp.where(
            mine, own[near, :].astype(f32), received[near, :].astype(f32)
        ).astype(bf16)

    ready(first_loads)
    cache_loads = [load(cache_values_hbm.at[s], cache_values.at[s]) for s in chunks]
    widened = tokens[...].astype(f32)
    normal_in = (normed(widened) * mix_gain[...]).astype(bf16)
    seq_row = lax.broadcasted_iota(jnp.int32, (seq_count, 128), 0)
    length = jnp.zeros((seq_count, 128), jnp.int32)
    for s in range(seq_count):
        length = jnp.where(seq_row == s, lengths_ref[s], length)
    lane = lax.broadcasted_iota(jnp.int32, (seq_count, key_size), 1)
    half_size = key_size // 2
    turn = lax.broadcasted_iota(jnp.int32, (1, key_size), 1) % half_size
    inverse = jnp.ones((1, key_size), f32)
    for i in range(1, half_size):
        inverse = jnp.where(turn == i, rope_base ** (-i / half_size), inverse)
    angles = length.astype(f32) * inverse
    cosine = jnp.cos(angles)
    sine = jnp.where(lane < key_size // 2, -1.0, 1.0) * jnp.sin(angles)
    filled_rows = lax.rem(length, block).astype(f32)

    def rotate(values):
        pieces = []
        for h in range(heads):
            piece = values[:, h * key_size : (h + 1) * key_size]
            pieces.append(piece * cosine + pltpu.roll(piece, key_size // 2, 1) * sine)
        return jnp.concatenate(pieces, axis=-1)

    raw_query = dot(normal_in, query_weight[...])
    raw_key = dot(normal_in, key_weight[...])
    query = (rotate(raw_query) * key_size ** (-0.5)).astype(bf16).astype(f32)
    new_key = rotate(raw_key).astype(bf16)
    new_keys_ref[...] = new_key
    queries[...] = query
    turned[...] = query.T
    new_key = new_key.astype(f32)
    own_weight = [
        jnp.sum(
            query[:, h * key_size : (h + 1) * key_size]
            * new_key[:, h * key_size : (h + 1) * key_size],
            axis=-1,
            keepdims=True,
        )
        .astype(bf16)
        .astype(f32)
        for h in range(heads)
    ]

    ready(dense_loads)
    pl.semaphore_wait(barrier, len(lines))
    spread_entry(entry_sem.at[0], y_ids)
    view = dense_weights.at[:, z, c]
    from_z = [copy(view, view, p) for p in z_ids]

    rates = [math.log1p(-(2.0 ** (-5 - h))) for h in range(heads)]
    head_row = lax.broadcasted_iota(jnp.int32, (8, heads * key_size), 0)
    head_lane = lax.broadcasted_iota(jnp.int32, (8, heads * key_size), 1)
    place_row = lax.broadcasted_iota(jnp.int32, (8, block), 0)
    place = lax.broadcasted_iota(jnp.int32, (8, block), 1)
    rate = jnp.zeros((8, block), f32)
    for h in range(heads):
        rate = jnp.where(place_row == h, rates[h], rate)
    of_head = head_lane // key_size == head_row
    state_loads = []
    for i, made in enumerate(key_loads):
        made.wait()
        state_loads.append(load(state_hbm.at[chunks[i]], state.at[chunks[i]]))
        for s in range(i * chunk, (i + 1) * chunk):
            spread = jnp.where(of_head, queries[s : s + 1, :], 0.0).astype(bf16)
            found = dot_rows(spread, cache_keys[s])
            filled = lax.rem(lengths_ref[s], block)
            distance = jnp.maximum(filled - place, 0).astype(f32)
            block_scores[s] = jnp.where(
                place < filled, found * jnp.exp(distance * rate), 0.0
            ).astype(bf16)

    pl.semaphore_wait(entry_sem.at[0], len(y_ids))
    spread_entry(entry_sem.at[1], z_ids)
    ready(value_loads)
    out_loads = [load(out_weight_hbm, out_weight), load(ffn_gain_hbm, ffn_gain)]
    new_value = dot(normal_in, value_weight[...]).astype(bf16)
    new_values_ref[...] = new_value

    value_row = lax.broadcasted_iota(jnp.int32, (8, model), 0)
    value_lane = lax.broadcasted_iota(jnp.int32, (8, model), 1)
    of_value = value_lane // value_size == value_row
    for i, made in enumerate(cache_loads):
        made.wait()
        for s in range(i * chunk, (i + 1) * chunk):
            found = dot(block_scores[s], cache_values[s])
            inside[s : s + 1, :] = jnp.sum(
                jnp.where(of_value, found, 0.0), axis=0, keepdims=True
            )

    expert_loads = [
        load(expert_gate_hbm.at[0], expert_gate),
        load(expert_up_hbm.at[0], expert_up),
        load(expert_down_hbm.at[0], expert_down),
        load(mix_hbm, mix),
    ]
    shared_loads = [
        load(shared_gate_hbm, shared_gate),
        load(shared_up_hbm, shared_up),
        load(shared_down_hbm, shared_down),
    ]
    ready(route_loads)
    pick, coarse, fine = slot_tables(routes[...], scores[...], count)

    for i, made in enumerate(state_loads):
        made.wait()
        for s in range(i * chunk, (i + 1) * chunk):
            for h in range(heads):
                weights = turned[h * key_size : (h + 1) * key_size, s : s + 1]
                carried[s : s + 1, h * value_size : (h + 1) * value_size] = jnp.sum(
                    state[s, h] * weights, axis=0, keepdims=True
                )

    headed = []
    for h in range(heads):
        span = slice(h * value_size, (h + 1) * value_size)
        decay = jnp.exp((filled_rows[:, :1] + 1.0) * rates[h])
        retained = (
            inside[:, span]
            + own_weight[h] * new_value[:, span].astype(f32)
            + decay * carried[:, span]
        )
        headed.append(normed(retained).astype(bf16))
    ready(out_loads)
    mixer_out = dot(jnp.concatenate(headed, axis=-1), out_weight[...])
    residual = widened + normed(mixer_out)
    features = (normed(residual) * ffn_gain[...]).astype(bf16)

    pl.semaphore_wait(entry_sem.at[1], len(z_ids))
    group_tokens[y, x] = features
    rows_out[...] = dot(pick, features).astype(bf16)

    first, last = pl.ds(0, part), pl.ds(part, part)
    view = group_tokens.at[y, x, :, first]
    gather_1a = [copy(view, view, p) for p in x_ids]
    view = group_tokens.at[y, x, :, last]
    gather_1b = [copy(view, view, p) for p in y_ids]
    exchange(rows_out, rows_in, 0)
    ready(shared_loads)
    shared_hidden = (silu(dot(features, shared_gate[...])) * dot(features, shared_up[...])).astype(
        bf16
    )
    shared_out = dot(shared_hidden, shared_down[...])
    arrive(from_z)
    view = dense_weights.at[:, :, c]
    from_core = [copy(view, view, core_id)]
    arrive(gather_1a)
    view = group_tokens.at[y, :, :, first]
    gather_2 = [copy(view, view, p) for p in y_ids]
    arrive(gather_1b)
    view = group_tokens.at[:, x, :, last]
    gather_2 += [copy(view, view, p) for p in x_ids]

    ready(expert_loads)
    everything(0).wait_recv()
    complete(rows_out, rows_in)
    inputs = rows_in[...]
    hidden = (silu(dot(inputs, expert_gate[...])) * dot(inputs, expert_up[...])).astype(bf16)
    answers_out[...] = dot(hidden, expert_down[...]).astype(bf16)
    exchange(answers_out, answers_in, 1)

    arrive(gather_2)
    arrive(from_core)
    units = nz * nc * dense_gate_hbm.shape[0]
    inputs = group_tokens[...].reshape(ny * nx * seq_count, model)
    hidden = (
        silu(dot_rows(inputs, dense_weights[0].reshape(units, model)))
        * dot_rows(inputs, dense_weights[1].reshape(units, model))
    ).astype(bf16)
    group_part[...] = (
        dot(hidden, dense_weights[2].reshape(units, model))
        .astype(bf16)
        .reshape(ny, nx, seq_count, model)
    )
    step = []
    for d, (p, peer) in enumerate(zip(y_peers, y_ids)):
        step.append(copy(group_part.at[p, :, :, first], in_1a.at[d], peer))
    for d, (p, peer) in enumerate(zip(x_peers, x_ids)):
        step.append(copy(group_part.at[:, p, :, last], in_1b.at[d], peer))

    def add(*terms):
        total = terms[0].astype(f32)
        for term in terms[1:]:
            total = total + term.astype(f32)
        return total

    arrive(step)
    sum_1a[...] = add(group_part[y, :, :, :part], *[in_1a[d] for d in range(ny - 1)]).astype(bf16)
    sum_1b[...] = add(group_part[:, x, :, part:], *[in_1b[d] for d in range(nx - 1)]).astype(bf16)
    step = []
    for d, (p, peer) in enumerate(zip(x_peers, x_ids)):
        step.append(copy(sum_1a.at[p], in_2a.at[d], peer))
    for d, (p, peer) in enumerate(zip(y_peers, y_ids)):
        step.append(copy(sum_1b.at[p], in_2b.at[d], peer))
    arrive(step)
    dense_out = jnp.concatenate(
        [
            add(sum_1a[x], *[in_2a[d] for d in range(nx - 1)]),
            add(sum_1b[y], *[in_2b[d] for d in range(ny - 1)]),
        ],
        axis=-1,
    )
    gate = 1.0 / (1.0 + jnp.exp(-mix[...]))
    combined = shared_out + gate * dense_out

    everything(1).wait_recv()
    complete(answers_out, answers_in)
    answers = answers_in[...]
    combined = combined + (dot(coarse, answers) + dot(fine, answers))
    out_ref[...] = (residual + normed(combined)).astype(bf16)
    for made in sent + [everything(0), everything(1)]:
        made.wait_send()


def hand_over(a_ref, b_ref, c_ref, a_out, b_out, c_out, sems):
    pairs = ((a_ref, a_out), (b_ref, b_out), (c_ref, c_out))
    moves = [pltpu.make_async_copy(*pair, sems.at[i]) for i, pair in enumerate(pairs)]
    for move in moves:
        move.start()
    for move in moves:
        move.wait()


def per_device(
    tokens,
    lengths,
    cache_keys,
    cache_values,
    retention_state,
    mix_gain,
    query_weight,
    key_weight,
    value_weight,
    out_weight,
    ffn_gain,
    routes,
    route_scores,
    expert_gate,
    expert_up,
    expert_down,
    shared_gate,
    shared_up,
    shared_down,
    dense_gate,
    dense_up,
    dense_down,
    dense_mix,
):
    count = lax.axis_size("ep")
    dims = grid_of(count)
    nz, ny, nx, nc = dims
    seq_count, model = tokens.shape
    heads, key_size, value_size = retention_state.shape[1:]
    block = cache_keys.shape[1]
    part = model // 2
    bf16 = jnp.bfloat16
    f32 = jnp.float32
    operands = (
        tokens,
        cache_keys,
        cache_values,
        retention_state,
        mix_gain[None, :],
        query_weight,
        key_weight,
        value_weight,
        out_weight,
        ffn_gain[None, :],
        routes.T,
        route_scores.T,
        expert_gate,
        expert_up,
        expert_down,
        shared_gate,
        shared_up,
        shared_down,
        dense_gate,
        dense_up,
        dense_down,
        dense_mix[None, :],
    )
    copies = 4 * (ny - 1) + 4 * (nx - 1) + (nz - 1) + 1

    def room(*shape):
        return pltpu.VMEM(shape, bf16)

    def like(array):
        return pltpu.VMEM(array.shape, array.dtype)

    rows = (2 * count, model)
    scratch = [
        like(tokens),
        like(cache_keys),
        like(cache_values),
        like(retention_state),
        pltpu.VMEM((1, model), f32),
        like(query_weight),
        like(key_weight),
        like(value_weight),
        like(out_weight),
        pltpu.VMEM((1, model), f32),
        pltpu.VMEM(routes.shape[::-1], routes.dtype),
        pltpu.VMEM(route_scores.shape[::-1], f32),
        pltpu.VMEM((1, model), f32),
        room(*expert_gate.shape[1:]),
        room(*expert_gate.shape[1:]),
        room(*expert_down.shape[1:]),
        like(shared_gate),
        like(shared_up),
        like(shared_down),
        room(3, nz, nc, *dense_gate.shape),
        pltpu.VMEM((seq_count, heads * key_size), f32),
        pltpu.VMEM((heads * key_size, seq_count), f32),
        room(seq_count, 8, block),
        pltpu.VMEM((seq_count, model), f32),
        pltpu.VMEM((seq_count, model), f32),
        room(*rows),
        room(*rows),
        room(*rows),
        room(*rows),
        room(2 * (count - 1) * model // 256, 256),
        room(ny, nx, seq_count, model),
        room(ny, nx, seq_count, model),
        room(ny - 1, nx, seq_count, part),
        room(nx - 1, ny, seq_count, part),
        room(nx, seq_count, part),
        room(ny, seq_count, part),
        room(nx - 1, seq_count, part),
        room(ny - 1, seq_count, part),
        pltpu.SemaphoreType.DMA((40,)),
        pltpu.SemaphoreType.DMA((copies,)),
        pltpu.SemaphoreType.DMA((copies,)),
        pltpu.SemaphoreType.DMA((2,)),
        pltpu.SemaphoreType.DMA((2,)),
        pltpu.SemaphoreType.REGULAR((2,)),
    ]
    vmem = pl.BlockSpec(memory_space=pltpu.VMEM)
    shapes = [(seq_count, model), (seq_count, heads * key_size), (seq_count, model)]
    made = pl.pallas_call(
        functools.partial(layer_kernel, dims),
        out_shape=tuple(pltpu.VMEM(shape, bf16) for shape in shapes),
        in_specs=[pl.BlockSpec(memory_space=pltpu.SMEM)]
        + [pl.BlockSpec(memory_space=pl.ANY)] * len(operands),
        out_specs=(vmem, vmem, vmem),
        scratch_shapes=scratch,
        compiler_params=pltpu.CompilerParams(
            collective_id=0, has_side_effects=True, vmem_limit_bytes=56 * 2**20
        ),
    )(lengths, *operands)
    return tuple(
        pl.pallas_call(
            hand_over,
            out_shape=tuple(jax.ShapeDtypeStruct(shape, bf16) for shape in shapes),
            in_specs=[vmem] * 3,
            out_specs=[pl.BlockSpec(memory_space=pl.ANY)] * 3,
            scratch_shapes=[pltpu.SemaphoreType.DMA((3,))],
        )(*[pltpu.with_memory_space_constraint(m, pltpu.VMEM) for m in made])
    )


def solution(mesh):
    in_specs = (
        P("ep", None),
        P("ep"),
        P("ep", None, None),
        P("ep", None, None),
        P("ep", None, None, None),
        P(),
        P(),
        P(),
        P(),
        P(),
        P(),
        P("ep", None),
        P("ep", None),
        P("ep", None, None),
        P("ep", None, None),
        P("ep", None, None),
        P(),
        P(),
        P(),
        P("ep", None),
        P("ep", None),
        P("ep", None),
        P(),
    )
    out_specs = (P("ep", None), P("ep", None), P("ep", None))
    return jax.shard_map(
        per_device, mesh=mesh, in_specs=in_specs, out_specs=out_specs, check_vma=False
    )
```

time: 73.3 us -> 44.2 us (0.60)
  matrix products: 15.4 us -> 0 us
  local copies, waits for them, and re-layouts: 7.37 us -> 0 us
  other arithmetic: 3.73 us -> 0 us
  Pallas kernels: 45.6 us -> 43.4 us
    dot_general x7 -> x0, matrix products: 15.4 us -> none  [the longest x1 6.26 us: retain(): jnp.einsum('shd,shde->she', queries.astype(jnp.float32), carry_state, pre...]
    reshape x3 -> x0, local copies, waits for them, and re-layouts: 3.94 us -> none  [the longest x1 3.91 us: retain(): cache_keys.reshape(seq_count, block_size, head_count, key_size)]
    unnamed x25 -> x0, local copies, waits for them, and re-layouts: 3.4 us -> none
    pallas_call x1 -> x2, Pallas kernels: 45.6 us -> 43.4 us  [the longest x1 42.8 us: per_device(): pl.pallas_call(functools.partial(layer_kernel, dims), out_shape=tuple((pl...]
    convert_element_type x6 -> x0, other arithmetic: 1.61 us -> none  [the longest x1 0.69 us: per_device(): features = (normed(residual) * ffn_gain).astype(jnp.bfloat16)]
    reduce_sum x4 -> x0, other arithmetic: 1.6 us -> none  [the longest x3 1.41 us: normed(): jnp.mean(values * values, axis=-1, keepdims=True) + eps]
where the time goes in v2:
time: 44.2 us; the launch traced here: 44.1 us
  Pallas kernels  43.4 us (98%)
  between operations  0.65 us (1%)
    pallas_call x1, Pallas kernels, per_device(): pl.pallas_call(functools.partial(layer_kernel, dims), out_shape=tuple((pl...  42.8 us

profile of v2, /device:TPU:0, one launch (start us, length us, event | category | flops | bytes accessed | tf_op | source)
XLA Modules:
  0.0 44.1 jit_solution(5702994671581140903)
XLA Ops:
  0.6 42.8 %shard_map.238 = (bf16[16,1024]{1,0:T(8,128)(2,1)S(1)}, bf16[16,512]{1,0:T(8,128)(2,1)S(1)}, bf16[16,1024]{1,0:T(8,128)(2,1)S(1)}) custom-call(s32[16]{0:T(128)} %lengths_ref.1, bf16[16,1024]{1,0:T(8,128)(2,1)} %tokens_hbm.1, bf16[16,128,512]{2,1,0:T(8,128)(2,1)} %cache_keys_hbm.1, bf16[16,128,1024]{2,1,0:T(8,128)(2,1)} %cache_values_hbm.1, ...), custom_call_target="tpu_custom_call" | custom-call | tf_op jit(solution)/shard_map/pallas_call | solution.py:614
  43.4 0.7 %shard_map.239 = (bf16[16,1024]{1,0:T(8,128)(2,1)}, bf16[16,512]{1,0:T(8,128)(2,1)}, bf16[16,1024]{1,0:T(8,128)(2,1)}) custom-call(bf16[16,1024]{1,0:T(8,128)(2,1)S(1)} %get-tuple-element.6.a_ref, bf16[16,512]{1,0:T(8,128)(2,1)S(1)} %get-tuple-element.7.b_ref, bf16[16,1024]{1,0:T(8,128)(2,1)S(1)} %get-tuple-element.8.c_ref), custom_call_target="tpu_custom_call" | custom-call | tf_op jit(solution)/shard_map/pallas_call | solution.py:626
